TPU v7x, 32 devices: a whole 2x2x4 slice. The times are simulated.
32 devices in a mesh: grp: 2 (over y), sp: 4 (over z), tp: 4 (over x, core).
Axes of the slice: x: 2, y: 2, z: 4, core: 2. Of those that a mesh axis runs over, the one named last changes fastest.
Arguments:
- stream: bfloat16 [12288, 4096], P(('grp', 'sp', 'tp')), parts along dimension 0, may hold values from -6 to 6
- norm_gain: float32 [2, 4096], replicated, may hold values from 0.1 to 1.9
- mix_weight: bfloat16 [2, 4, 1024, 1024], P(None, None, 'sp', 'tp'), may hold values from -0.1875 to 0.1875
- branch_scale: float32 [2, 4096], replicated, may hold values from 0.1 to 1.9
Outputs:
- result: bfloat16 [12288, 4096], P(('grp', 'sp', 'tp')), parts along dimension 0
There are 2 independent parts, one for each index of `grp`. A program takes and returns all parts, laid end to end along the dimension named above; an argument that names none is the same for every part. Nothing has to cross between parts.
All inputs are finite; a program needn't handle non-finite values.
Results may differ from a plain program's by a relative error of at most 0.0056.
Values may be sent and summed in bfloat16 or wider, within the bound.
A program may use at most 128 MiB of HBM per device.

v0:
```python
import jax
import jax.numpy as jnp
from jax import lax
from jax.sharding import PartitionSpec as P

GW = 1024
G = 4
LAYERS = 2
epsilon = 1e-06
window_lengths = (2, 4, 8, 16)
halo_rows = 15


def from_behind(block, axis, distance):
    devices = range(lax.axis_size(axis))
    route = [(i - distance, i) for i in devices if i - distance in devices]
    return lax.ppermute(block, axis, route)


def per_device(stream, norm_gain, mix_weight, branch_scale):
    row_count = stream.shape[0]
    feature_width = stream.shape[1]
    offset = lax.axis_index(("sp", "tp")) * row_count
    counts_base = (offset + lax.iota(jnp.int32, row_count)).astype(jnp.float32) + 1.0
    residual = stream.astype(jnp.float32)
    for layer_idx in range(LAYERS):
        scale_rows = lax.rsqrt(jnp.mean(residual * residual, axis=1, keepdims=True) + epsilon)
        normed = (residual * scale_rows * norm_gain[layer_idx]).astype(jnp.bfloat16)
        earlier = from_behind(normed[row_count - halo_rows :], ("sp", "tp"), 1)
        extended = jnp.concatenate([earlier, normed], axis=0).astype(jnp.float32)
        pieces = []
        for group_idx in range(G):
            window_len = window_lengths[group_idx]
            segment = extended[:, group_idx * GW : (group_idx + 1) * GW]
            own_rows = segment[halo_rows:]
            running = own_rows
            for back_step in range(1, window_len):
                running = (
                    running + segment[halo_rows - back_step : halo_rows - back_step + row_count]
                )
            window_mean = running / jnp.minimum(counts_base, float(window_len))[:, None]
            pieces.append((window_mean - own_rows).astype(jnp.bfloat16))
        pooled = jnp.stack(pieces, axis=1)
        weight_shard = mix_weight[layer_idx]
        full_rows = lax.all_gather(weight_shard, "sp", axis=1, tiled=True)
        mixed_out = jnp.einsum(
            "rgc,gcn->rgn",
            pooled,
            lax.all_gather(full_rows, "tp", axis=2, tiled=True),
            preferred_element_type=jnp.float32,
        )
        residual = residual + mixed_out.reshape(row_count, feature_width) * branch_scale[layer_idx]
    return residual.astype(jnp.bfloat16)


def solution(mesh):
    return jax.shard_map(
        per_device,
        mesh=mesh,
        in_specs=(P(("grp", "sp", "tp"), None), P(), P(None, None, "sp", "tp"), P()),
        out_specs=P(("grp", "sp", "tp"), None),
        check_vma=False,
    )
```

profile of v0, /device:TPU:9, one launch (start us, length us, event | category | flops | bytes accessed | tf_op | source)
XLA Modules:
  0.0 248.3 jit_solution(16958773101239605890)
XLA Ops:
  6.5 0.0 all-gather.9.cloned.1.call-start
  6.5 2.2 fusion.69
  8.8 0.0 copy-start.1
  8.8 0.0 all-gather.9.cloned.1.call-update
  8.8 0.0 all-gather.13.cloned.1.call-start
  8.9 0.7 all-gather.13.cloned.1.call-update
  9.6 0.0 all-gather.11.cloned.1.call-start
  9.6 44.4 %all-gather.9.cloned.1.call-done = bf16[1,4,1024,256]{3,2,1,0:T(8,128)(2,1)} async-done(((bf16[1,4,256,256]{3,2,1,0:T(8,128)(2,1)}), bf16[1,4,1024,256]{3,2,1,0:T(8,128)(2,1)}) %all-gather.9.cloned.1.call-update) | async-done | bytes 2097168 | tf_op jit(solution)/shard_map/all_gather | solution.py:45
  54.0 0.0 all-gather.11.cloned.1.call-update
  54.0 0.0 all-gather.15.cloned.1.call-start
  54.0 0.0 copy-done.1
  54.0 0.7 fusion.4
  54.7 0.0 copy-start.3
  54.8 45.3 %all-gather.13.cloned.1.call-done = bf16[1,4,1024,256]{3,2,1,0:T(8,128)(2,1)} async-done(((bf16[1,4,256,256]{3,2,1,0:T(8,128)(2,1)}), bf16[1,4,1024,256]{3,2,1,0:T(8,128)(2,1)}) %all-gather.13.cloned.1.call-update) | async-done | bytes 2097168 | tf_op jit(solution)/shard_map/all_gather | solution.py:45
  100.0 0.0 all-gather.15.cloned.1.call-update
  100.0 0.0 copy-done.3
  100.1 0.0 copy-start.4
  100.1 1.0 fusion.6
  101.1 0.0 copy-start.2
  101.1 1.7 copy-done.2
  102.8 4.2 %collective-permute-start = (bf16[15,4096]{1,0:T(8,128)(2,1)S(1)}, bf16[15,4096]{1,0:T(8,128)(2,1)S(1)}, u32[]{:S(2)}, u32[]{:S(2)}) collective-permute-start(bf16[15,4096]{1,0:T(8,128)(2,1)S(1)} %slice.340), channel_id=1, source_target_pairs={{0,1},{1,2},{2,3},{3,4},{4,5},{5,6},{6,7},{7,8},{8,9},{9,10},{10,1... | collective-permute-start | bytes 368648 | tf_op jit(solution)/shard_map/ppermute | solution.py:17
  107.0 0.0 copy-done.4
  107.1 1.8 collective-permute-done
  108.9 3.2 %maximum_convert_fusion = f32[399,4096]{1,0:T(8,128)S(1)} fusion(bf16[384,4096]{1,0:T(8,128)(2,1)} %copy-done.2, bf16[15,4096]{1,0:T(8,128)(2,1)S(1)} %collective-permute-done), kind=kLoop, calls=%fused_computation.13 | loop fusion | flops 6537216 | bytes 9805824 | tf_op jit(solution)/shard_map/convert_element_type | solution.py:30
  112.2 3.3 %fusion.62 = bf16[384,1,1024]{2,0,1:T(8,128)(2,1)} fusion(f32[384]{0:T(512)S(1)} %fusion.63, f32[399,4096]{1,0:T(8,128)S(1)} %maximum_convert_fusion), kind=kLoop, calls=%fused_computation.114 | loop fusion | flops 7077888 | bytes 25953792 | tf_op jit(solution)/shard_map/stack | solution.py:43
  115.4 3.6 %fusion.56 = (bf16[384,1,1024]{2,0,1:T(8,128)(2,1)}, bf16[384,1,1024]{2,0,1:T(8,128)(2,1)}, bf16[384,1,1024]{2,0,1:T(8,128)(2,1)}) fusion(f32[384]{0:T(512)S(1)} %fusion.66, f32[399,4096]{1,0:T(8,128)S(1)} %maximum_convert_fusion, f32[384]{0:T(512)S(1)} %get-tuple-element.18, f32[384]{0:T(512)S(1)} %get-tuple-element.17), kind=kLoop, calls=%fused_computation.108 | loop fusion | flops 7864320 | bytes 24384000 | tf_op jit(solution)/shard_map/stack | solution.py:43
  119.0 43.0 %all-gather.11.cloned.1.call-done = bf16[1,4,1024,1024]{3,2,1,0:T(8,128)(2,1)} async-done(((bf16[1,4,1024,256]{3,2,1,0:T(8,128)(2,1)}), bf16[1,4,1024,1024]{3,2,1,0:T(8,128)(2,1)}) %all-gather.11.cloned.1.call-update) | async-done | bytes 8388624 | tf_op jit(solution)/shard_map/all_gather | solution.py:49
  162.0 7.8 %fusion.21 = f32[4,48,8,1024]{3,2,1,0:T(8,128)S(1)} fusion(bf16[1,4,1024,1024]{3,2,1,0:T(8,128)(2,1)} %all-gather.11.cloned.1.call-done, bf16[384,1,1024]{2,0,1:T(8,128)(2,1)} %fusion.62, bf16[384,1,1024]{2,0,1:T(8,128)(2,1)} %get-tuple-element.10, bf16[384,1,1024]{2,0,1:T(8,128)(2,1)} %get-tuple-element.9, bf16[384,1,1024]{2,0,1:T(8,128)(2,1)} %get-tuple-element.8), kind=kOutput, calls=%fused_computation.29 | convolution fusion | flops 3225944064 | bytes 17825792 | tf_op jit(solution)/shard_map/rgc,gcn->rgn/dot_general | solution.py:46
  169.8 0.6 copy.7
  170.4 0.0 copy-start
  170.4 1.2 multiply_reduce_fusion
  171.6 2.0 copy-done
  173.7 1.6 multiply_convert_fusion
  175.3 2.3 collective-permute-start.1
  177.6 4.6 %collective-permute-done.1 = bf16[15,4096]{1,0:T(8,128)(2,1)S(1)} collective-permute-done((bf16[15,4096]{1,0:T(8,128)(2,1)S(1)}, bf16[15,4096]{1,0:T(8,128)(2,1)S(1)}, u32[]{:S(2)}, u32[]{:S(2)}) %collective-permute-start.1) | collective-permute-done | bytes 122912 | tf_op jit(solution)/shard_map/ppermute | solution.py:17
  182.2 0.9 maximum_convert_fusion.1
  183.1 3.3 %fusion.61 = bf16[384,1,1024]{2,0,1:T(8,128)(2,1)} fusion(f32[384]{0:T(512)S(1)} %fusion.63, f32[399,4096]{1,0:T(8,128)S(1)} %maximum_convert_fusion.1), kind=kLoop, calls=%fused_computation.113 | loop fusion | flops 7077888 | bytes 25953792 | tf_op jit(solution)/shard_map/stack | solution.py:43
  186.4 3.5 %fusion.55 = (bf16[384,1,1024]{2,0,1:T(8,128)(2,1)}, bf16[384,1,1024]{2,0,1:T(8,128)(2,1)}, bf16[384,1,1024]{2,0,1:T(8,128)(2,1)}) fusion(f32[384]{0:T(512)S(1)} %fusion.66, f32[399,4096]{1,0:T(8,128)S(1)} %maximum_convert_fusion.1, f32[384]{0:T(512)S(1)} %get-tuple-element.18, f32[384]{0:T(512)S(1)} %get-tuple-element.17), kind=kLoop, calls=%fused_computation.107 | loop fusion | flops 7864320 | bytes 24384000 | tf_op jit(solution)/shard_map/stack | solution.py:43
  189.9 34.3 %all-gather.15.cloned.1.call-done = bf16[1,4,1024,1024]{3,2,1,0:T(8,128)(2,1)} async-done(((bf16[1,4,1024,256]{3,2,1,0:T(8,128)(2,1)}), bf16[1,4,1024,1024]{3,2,1,0:T(8,128)(2,1)}) %all-gather.15.cloned.1.call-update) | async-done | bytes 8388624 | tf_op jit(solution)/shard_map/all_gather | solution.py:49
  224.3 0.0 slice-start
  224.3 0.0 slice-start.1
  224.3 7.9 %fusion.26 = f32[4,48,8,1024]{3,2,1,0:T(8,128)S(1)} fusion(bf16[1,4,1024,1024]{3,2,1,0:T(8,128)(2,1)} %all-gather.15.cloned.1.call-done, bf16[384,1,1024]{2,0,1:T(8,128)(2,1)} %fusion.61, bf16[384,1,1024]{2,0,1:T(8,128)(2,1)} %get-tuple-element.7, bf16[384,1,1024]{2,0,1:T(8,128)(2,1)} %get-tuple-element.6, bf16[384,1,1024]{2,0,1:T(8,128)(2,1)} %get-tuple-element.5), kind=kOutput, calls=%fused_computation.30 | convolution fusion | flops 3225944064 | bytes 17825792 | tf_op jit(solution)/shard_map/rgc,gcn->rgn/dot_general | solution.py:46
  232.2 3.4 %copy.8 = f32[4,48,8,1024]{3,2,0,1:T(8,128)} copy(f32[4,48,8,1024]{3,2,1,0:T(8,128)S(1)} %fusion.26) | data formatting | bytes 12582912 | tf_op jit(solution)/shard_map/reshape | solution.py:52
  235.6 0.0 slice-done
  235.6 0.0 slice-done.1
  235.6 6.2 %add_convert_fusion = bf16[384,4096]{1,0:T(8,128)(2,1)} fusion(f32[384,4096]{1,0:T(8,128)} %bitcast.43, f32[4096]{0:T(1024)S(1)} %bitcast.47, f32[384,4096]{1,0:T(8,128)S(1)} %bitcast.42, f32[4096]{0:T(1024)S(1)} %bitcast.46, bf16[384,4096]{1,0:T(8,128)(2,1)S(1)} %copy-done.1), kind=kLoop, calls=%fused_computation.10 | loop fusion | flops 9437184 | bytes 18907136 | tf_op jit(solution)/shard_map/convert_element_type | solution.py:53
  (10 shorter events, 0.2 us)
Async XLA Ops:
  6.5 47.4 %all-gather.9.cloned.1.call-start = ((), (), s32[]{:S(2)}) async-start(), calls=%async_computation | async-start | bytes 2621440 | tf_op jit(solution)/shard_map/all_gather | solution.py:45
  8.8 45.3 %copy-start.1 = (bf16[384,4096]{1,0:T(8,128)(2,1)S(1)}, bf16[384,4096]{1,0:T(8,128)(2,1)}, u32[]{:S(2)}) copy-start(bf16[384,4096]{1,0:T(8,128)(2,1)} %param.4) | copy-start | bytes 9437188
  8.8 91.2 %all-gather.13.cloned.1.call-start = ((), (), s32[]{:S(2)}) async-start(), calls=%async_computation.2 | async-start | bytes 2621440 | tf_op jit(solution)/shard_map/all_gather | solution.py:45
  9.6 152.5 %all-gather.11.cloned.1.call-start = ((), (), s32[]{:S(2)}) async-start(), calls=%async_computation.1 | async-start | bytes 10485760 | tf_op jit(solution)/shard_map/all_gather | solution.py:49
  54.0 170.3 %all-gather.15.cloned.1.call-start = ((), (), s32[]{:S(2)}) async-start(), calls=%async_computation.3 | async-start | bytes 10485760 | tf_op jit(solution)/shard_map/all_gather | solution.py:49
  54.7 45.3 %copy-start.3 = (f32[2,4096]{1,0:T(2,128)S(1)}, f32[2,4096]{1,0:T(2,128)}, u32[]{:S(2)}) copy-start(f32[2,4096]{1,0:T(2,128)} %param.5) | copy-start | bytes 98308
  100.1 6.9 %copy-start.4 = (f32[2,4096]{1,0:T(2,128)S(1)}, f32[2,4096]{1,0:T(2,128)}, u32[]{:S(2)}) copy-start(f32[2,4096]{1,0:T(2,128)} %param.7) | copy-start | bytes 98308
  101.1 1.7 copy-start.2
  102.8 6.1 %collective-permute-start = (bf16[15,4096]{1,0:T(8,128)(2,1)S(1)}, bf16[15,4096]{1,0:T(8,128)(2,1)S(1)}, u32[]{:S(2)}, u32[]{:S(2)}) collective-permute-start(bf16[15,4096]{1,0:T(8,128)(2,1)S(1)} %slice.340), channel_id=1, source_target_pairs={{0,1},{1,2},{2,3},{3,4},{4,5},{5,6},{6,7},{7,8},{8,9},{9,10},{10,1... | collective-permute-start | bytes 368648 | tf_op jit(solution)/shard_map/ppermute | solution.py:17
  170.4 3.3 %copy-start = (f32[4,48,8,1024]{3,2,0,1:T(8,128)}, f32[4,48,8,1024]{3,2,0,1:T(8,128)S(1)}, u32[]{:S(2)}) copy-start(f32[4,48,8,1024]{3,2,0,1:T(8,128)S(1)} %copy.7) | copy-start | bytes 18874372
  175.3 6.9 %collective-permute-start.1 = (bf16[15,4096]{1,0:T(8,128)(2,1)S(1)}, bf16[15,4096]{1,0:T(8,128)(2,1)S(1)}, u32[]{:S(2)}, u32[]{:S(2)}) collective-permute-start(bf16[15,4096]{1,0:T(8,128)(2,1)S(1)} %slice.371), channel_id=1, source_target_pairs={{0,1},{1,2},{2,3},{3,4},{4,5},{5,6},{6,7},{7,8},{8,9},{9,10},{10,1... | collective-permute-start | bytes 368648 | tf_op jit(solution)/shard_map/ppermute | solution.py:17
  224.3 11.3 %slice-start = ((s8[6291456]{0:T(1024)(128)(4,1)}), s8[4194304]{0:T(1024)(128)(4,1)S(1)}, s32[]{:S(2)}) async-start(s8[6291456]{0:T(1024)(128)(4,1)} %bitcast.40), calls=%async_computation.4 | async-start | bytes 8388608
  224.3 11.3 %slice-start.1 = ((s8[6291456]{0:T(1024)(128)(4,1)}), s8[2097152]{0:T(1024)(128)(4,1)S(1)}, s32[]{:S(2)}) async-start(s8[6291456]{0:T(1024)(128)(4,1)} %bitcast.40), calls=%async_computation.5 | async-start | bytes 4194304
Sparse Core Ops, SparseCore 0:
  8.9 44.9 all-gather.8
  55.5 44.4 all-gather.12
  101.6 60.4 all-gather.10
  163.4 60.7 all-gather.14
where the time goes:
time: 249 us; the launch traced here: 248 us
  waiting for transfers between devices  174 us (70%)
  other arithmetic  28.5 us (11%)
  matrix products  15.6 us (6%)
  between operations  13.3 us (5%)
  local copies, waits for them, and re-layouts  10.1 us (4%)
  starting transfers between devices  6.56 us (3%)
    all_gather x2, waiting for transfers between devices, per_device(): full_rows = lax.all_gather(weight_shard, 'sp', axis=1, tiled=True)  89.6 us
    all_gather x2, waiting for transfers between devices, per_device(): lax.all_gather(full_rows, 'tp', axis=2, tiled=True)  77.3 us
    dot_general x2, matrix products, per_device(): jnp.einsum('rgc,gcn->rgn', pooled, lax.all_gather(full_rows, 'tp', axis=2...  15.6 us
    another operation x4, other arithmetic, per_device(): pooled = jnp.stack(pieces, axis=1)  13.6 us
    ppermute x2, waiting for transfers between devices, from_behind(): return lax.ppermute(block, axis, route)  6.48 us
    ppermute x2, starting transfers between devices, from_behind(): return lax.ppermute(block, axis, route)  6.44 us
    convert_element_type x1, other arithmetic, per_device(): return residual.astype(jnp.bfloat16)  6.2 us
  transfers between devices with their start and end apart: 6, of which 6 were waited for; matrix products, arithmetic and copies ran while one was open for 12% of the time, Pallas kernels for 0%

commit v1 on v0

--- a/solution.py
+++ b/solution.py
@@ -46,7 +46,7 @@
         mixed_out = jnp.einsum(
             "rgc,gcn->rgn",
             pooled,
-            lax.all_gather(full_rows, "tp", axis=2, tiled=True),
+            jnp.concatenate(lax.all_gather(full_rows, axis_name="tp"), axis=2),
             preferred_element_type=jnp.float32,
         )
         residual = residual + mixed_out.reshape(row_count, feature_width) * branch_scale[layer_idx]

time: 249 us -> 256 us (1.028)
  local copies, waits for them, and re-layouts: 10.1 us -> 27.1 us
  matrix products: 15.6 us -> 11.1 us
  waiting for transfers between devices: 174 us -> 171 us
    reshape x0 -> x2, local copies, waits for them, and re-layouts: none -> 15.9 us  [per_device(): jnp.concatenate(lax.all_gather(full_rows, axis_name='tp'), axis=2)]
    ppermute x2, waiting for transfers between devices: 6.48 us -> 1.84 us  [from_behind(): return lax.ppermute(block, axis, route)]
    dot_general x2, matrix products: 15.6 us -> 11.1 us  [per_device(): jnp.einsum('rgc,gcn->rgn', pooled, jnp.concatenate(lax.all_gather(full_ro...]
  transfers between devices with their start and end apart: 6 -> 6, of which waited for: 6 -> 5; matrix products, arithmetic and copies ran while one was open for 12% -> 15% of each run, Pallas kernels for 0% -> 0%
where the time goes in v1:
time: 256 us
  waiting for transfers between devices  171 us (67%)
  local copies, waits for them, and re-layouts  27.1 us (11%)
  other arithmetic  27.1 us (11%)
  between operations  13.4 us (5%)
  matrix products  11.1 us (4%)
  starting transfers between devices  6.73 us (3%)
    all_gather x2, waiting for transfers between devices, per_device(): full_rows = lax.all_gather(weight_shard, 'sp', axis=1, tiled=True)  90.3 us
    all_gather x2, waiting for transfers between devices, per_device(): lax.all_gather(full_rows, axis_name='tp')  77.7 us
    reshape x2, local copies, waits for them, and re-layouts, per_device(): jnp.concatenate(lax.all_gather(full_rows, axis_name='tp'), axis=2)  15.9 us
    another operation x4, other arithmetic, per_device(): pooled = jnp.stack(pieces, axis=1)  12.1 us
    dot_general x2, matrix products, per_device(): jnp.einsum('rgc,gcn->rgn', pooled, jnp.concatenate(lax.all_gather(full_ro...  11.1 us
    ppermute x2, starting transfers between devices, from_behind(): return lax.ppermute(block, axis, route)  6.61 us
    convert_element_type x1, other arithmetic, per_device(): return residual.astype(jnp.bfloat16)  6.2 us
  transfers between devices with their start and end apart: 6, of which 5 were waited for; matrix products, arithmetic and copies ran while one was open for 15% of the time, Pallas kernels for 0%

profile of v1, /device:TPU:9, one launch (start us, length us, event | category | flops | bytes accessed | tf_op | source)
XLA Modules:
  0.0 256.0 jit_solution(15359959572065421662)
XLA Ops:
  6.5 0.0 all-gather.9.cloned.1.call-start
  6.5 2.3 fusion.63
  8.8 0.0 all-gather.9.cloned.1.call-update
  8.8 0.0 all-gather.13.cloned.1.call-start
  8.9 0.7 all-gather.13.cloned.1.call-update
  9.6 0.0 all-gather.11.cloned.1.call-start
  9.6 44.4 %all-gather.9.cloned.1.call-done = bf16[1,4,1024,256]{3,2,1,0:T(8,128)(2,1)} async-done(((bf16[1,4,256,256]{3,2,1,0:T(8,128)(2,1)}), bf16[1,4,1024,256]{3,2,1,0:T(8,128)(2,1)}) %all-gather.9.cloned.1.call-update) | async-done | bytes 2097168 | tf_op jit(solution)/shard_map/all_gather | solution.py:45
  54.0 0.0 copy-start.1
  54.0 0.0 all-gather.11.cloned.1.call-update
  54.0 0.0 all-gather.15.cloned.1.call-start
  54.0 46.0 %all-gather.13.cloned.1.call-done = bf16[1,4,1024,256]{3,2,1,0:T(8,128)(2,1)} async-done(((bf16[1,4,256,256]{3,2,1,0:T(8,128)(2,1)}), bf16[1,4,1024,256]{3,2,1,0:T(8,128)(2,1)}) %all-gather.13.cloned.1.call-update) | async-done | bytes 2097168 | tf_op jit(solution)/shard_map/all_gather | solution.py:45
  100.0 0.0 all-gather.15.cloned.1.call-update
  100.1 0.0 copy-done.1
  100.1 0.0 copy-start.9
  100.1 0.7 fusion
  100.8 0.0 copy-done.9
  100.9 0.0 copy-start.10
  100.9 1.0 fusion.2
  101.9 0.0 copy-start.2
  101.9 1.7 copy-done.2
  103.6 4.2 %collective-permute-start = (bf16[15,4096]{1,0:T(8,128)(2,1)S(1)}, bf16[15,4096]{1,0:T(8,128)(2,1)S(1)}, u32[]{:S(2)}, u32[]{:S(2)}) collective-permute-start(bf16[15,4096]{1,0:T(8,128)(2,1)S(1)} %slice.340), channel_id=1, source_target_pairs={{0,1},{1,2},{2,3},{3,4},{4,5},{5,6},{6,7},{7,8},{8,9},{9,10},{10,1... | collective-permute-start | bytes 368648 | tf_op jit(solution)/shard_map/ppermute | solution.py:17
  107.8 0.0 copy-done.10
  107.8 1.8 collective-permute-done
  109.7 3.3 %maximum_convert_fusion = f32[399,4096]{1,0:T(8,128)S(1)} fusion(bf16[384,4096]{1,0:T(8,128)(2,1)} %copy-done.2, bf16[15,4096]{1,0:T(8,128)(2,1)S(1)} %collective-permute-done), kind=kLoop, calls=%fused_computation.9 | loop fusion | flops 6537216 | bytes 9805824 | tf_op jit(solution)/shard_map/convert_element_type | solution.py:30
  113.0 3.3 %fusion.56 = bf16[384,1,1024]{2,0,1:T(8,128)(2,1)} fusion(f32[384]{0:T(512)S(1)} %fusion.57, f32[399,4096]{1,0:T(8,128)S(1)} %maximum_convert_fusion), kind=kLoop, calls=%fused_computation.112 | loop fusion | flops 7077888 | bytes 25953792 | tf_op jit(solution)/shard_map/stack | solution.py:43
  116.3 3.6 %fusion.50 = (bf16[384,1,1024]{2,0,1:T(8,128)(2,1)}, bf16[384,1,1024]{2,0,1:T(8,128)(2,1)}, bf16[384,1,1024]{2,0,1:T(8,128)(2,1)}) fusion(f32[384]{0:T(512)S(1)} %fusion.60, f32[399,4096]{1,0:T(8,128)S(1)} %maximum_convert_fusion, f32[384]{0:T(512)S(1)} %get-tuple-element.18, f32[384]{0:T(512)S(1)} %get-tuple-element.17), kind=kLoop, calls=%fused_computation.106 | loop fusion | flops 7864320 | bytes 24384000 | tf_op jit(solution)/shard_map/stack | solution.py:43
  119.8 41.1 %all-gather.11.cloned.1.call-done = bf16[4,4,1024,256]{3,2,1,0:T(8,128)(2,1)} async-done(((bf16[1,4,1024,256]{3,2,1,0:T(8,128)(2,1)}), bf16[4,4,1024,256]{3,2,1,0:T(8,128)(2,1)}) %all-gather.11.cloned.1.call-update) | async-done | bytes 8388624 | tf_op jit(solution)/shard_map/all_gather | solution.py:49
  160.9 0.0 copy-start.5
  160.9 0.0 copy-start.6
  160.9 0.0 copy-start.7
  160.9 0.0 copy-start.8
  160.9 8.0 %copy.13 = bf16[4,4,128,8,256]{4,3,0,2,1:T(8,128)(2,1)} copy(bf16[4,4,128,8,256]{4,3,2,1,0:T(8,128)(2,1)} %bitcast.43) | data formatting | bytes 16777216 | tf_op jit(solution)/shard_map/reshape | solution.py:49
  168.9 0.0 copy-done.5
  168.9 0.0 copy-done.6
  168.9 0.0 copy-done.7
  168.9 0.0 copy-done.8
  168.9 7.6 %fusion.22 = f32[4,48,8,1024]{3,2,1,0:T(8,128)S(1)} fusion(bf16[4,1024,1024]{2,1,0:T(8,128)(2,1)} %bitcast.47, bf16[384,1,1024]{2,0,1:T(8,128)(2,1)S(1)} %copy-done.5, bf16[384,1,1024]{2,0,1:T(8,128)(2,1)S(1)} %copy-done.8, bf16[384,1,1024]{2,0,1:T(8,128)(2,1)S(1)} %copy-done.7, bf16[384,1,1024]{2,0,1:T(8,128)(2,1)S(1)} %copy-done.6), kind=kOutput, calls=%fused_computation.28 | convolution fusion | flops 3225944064 | bytes 17825792 | tf_op jit(solution)/shard_map/rgc,gcn->rgn/dot_general | solution.py:46
  176.5 0.6 copy.14
  177.1 0.0 copy-start
  177.1 1.2 multiply_reduce_fusion
  178.3 1.4 copy-done
  179.7 1.6 multiply_convert_fusion
  181.3 0.0 copy-start.3
  181.3 1.7 copy-done.3
  183.0 2.4 collective-permute-start.1
  185.4 36.6 %all-gather.15.cloned.1.call-done = bf16[4,4,1024,256]{3,2,1,0:T(8,128)(2,1)} async-done(((bf16[1,4,1024,256]{3,2,1,0:T(8,128)(2,1)}), bf16[4,4,1024,256]{3,2,1,0:T(8,128)(2,1)}) %all-gather.15.cloned.1.call-update) | async-done | bytes 8388624 | tf_op jit(solution)/shard_map/all_gather | solution.py:49
  222.0 0.0 copy-start.4
  222.0 7.9 %copy.15 = bf16[4,4,128,8,256]{4,3,0,2,1:T(8,128)(2,1)} copy(bf16[4,4,128,8,256]{4,3,2,1,0:T(8,128)(2,1)} %bitcast.42) | data formatting | bytes 16777216 | tf_op jit(solution)/shard_map/reshape | solution.py:49
  230.0 0.0 collective-permute-done.1
  230.0 0.0 copy-done.4
  230.0 0.9 maximum_convert_fusion.1
  230.9 0.0 slice-start.2
  230.9 2.8 %fusion.49 = (bf16[384,1,1024]{2,0,1:T(8,128)(2,1)S(1)}, bf16[384,1,1024]{2,0,1:T(8,128)(2,1)S(1)}, bf16[384,1,1024]{2,0,1:T(8,128)(2,1)S(1)}) fusion(f32[384]{0:T(512)S(1)} %fusion.60, f32[399,4096]{1,0:T(8,128)S(1)} %maximum_convert_fusion.1, f32[384]{0:T(512)S(1)} %get-tuple-element.18, f32[384]{0:T(512)S(1)} %get-tuple-element.17), kind=kLoop, calls=%fused_computation.105 | loop fusion | flops 7864320 | bytes 24384000 | tf_op jit(solution)/shard_map/stack | solution.py:43
  233.7 0.0 slice-start.3
  233.7 2.5 fusion.55
  236.3 0.0 slice-start
  236.3 0.0 slice-done.2
  236.3 0.0 slice-done.3
  236.3 0.0 slice-start.1
  236.3 3.5 %fusion.19 = f32[4,48,8,1024]{3,2,1,0:T(8,128)S(1)} fusion(bf16[4,1024,1024]{2,1,0:T(8,128)(2,1)S(1)} %bitcast.46, bf16[384,1,1024]{2,0,1:T(8,128)(2,1)S(1)} %fusion.55, bf16[384,1,1024]{2,0,1:T(8,128)(2,1)S(1)} %get-tuple-element.7, bf16[384,1,1024]{2,0,1:T(8,128)(2,1)S(1)} %get-tuple-element.6, bf16[384,1,1024]{2,0,1:T(8,128)(2,1)S(1)} %get-tuple-element.5), kind=kOutput, calls=%fused_computation.27 | convolution fusion | flops 3225944064 | bytes 17825792 | tf_op jit(solution)/shard_map/rgc,gcn->rgn/dot_general | solution.py:46
  239.8 3.4 %copy.16 = f32[4,48,8,1024]{3,2,0,1:T(8,128)} copy(f32[4,48,8,1024]{3,2,1,0:T(8,128)S(1)} %fusion.19) | data formatting | bytes 12582912 | tf_op jit(solution)/shard_map/reshape | solution.py:52
  243.2 0.0 slice-done
  243.2 0.0 slice-done.1
  243.2 6.2 %add_convert_fusion = bf16[384,4096]{1,0:T(8,128)(2,1)} fusion(f32[384,4096]{1,0:T(8,128)} %bitcast.41, f32[4096]{0:T(1024)S(1)} %bitcast.51, f32[384,4096]{1,0:T(8,128)S(1)} %bitcast.40, f32[4096]{0:T(1024)S(1)} %bitcast.50, bf16[384,4096]{1,0:T(8,128)(2,1)S(1)} %copy-done.1), kind=kLoop, calls=%fused_computation.6 | loop fusion | flops 9437184 | bytes 18907136 | tf_op jit(solution)/shard_map/convert_element_type | solution.py:53
  (11 shorter events, 0.2 us)
Async XLA Ops:
  6.5 47.4 %all-gather.9.cloned.1.call-start = ((), (), s32[]{:S(2)}) async-start(), calls=%async_computation | async-start | bytes 2621440 | tf_op jit(solution)/shard_map/all_gather | solution.py:45
  8.8 91.2 %all-gather.13.cloned.1.call-start = ((), (), s32[]{:S(2)}) async-start(), calls=%async_computation.2 | async-start | bytes 2621440 | tf_op jit(solution)/shard_map/all_gather | solution.py:45
  9.6 151.4 %all-gather.11.cloned.1.call-start = ((), (), s32[]{:S(2)}) async-start(), calls=%async_computation.1 | async-start | bytes 10485760 | tf_op jit(solution)/shard_map/all_gather | solution.py:49
  54.0 46.1 %copy-start.1 = (bf16[384,4096]{1,0:T(8,128)(2,1)S(1)}, bf16[384,4096]{1,0:T(8,128)(2,1)}, u32[]{:S(2)}) copy-start(bf16[384,4096]{1,0:T(8,128)(2,1)} %param.4) | copy-start | bytes 9437188
  54.0 168.0 %all-gather.15.cloned.1.call-start = ((), (), s32[]{:S(2)}) async-start(), calls=%async_computation.3 | async-start | bytes 10485760 | tf_op jit(solution)/shard_map/all_gather | solution.py:49
  100.1 0.8 copy-start.9
  100.9 6.9 %copy-start.10 = (f32[2,4096]{1,0:T(2,128)S(1)}, f32[2,4096]{1,0:T(2,128)}, u32[]{:S(2)}) copy-start(f32[2,4096]{1,0:T(2,128)} %param.7) | copy-start | bytes 98308
  101.9 1.7 copy-start.2
  103.6 6.1 %collective-permute-start = (bf16[15,4096]{1,0:T(8,128)(2,1)S(1)}, bf16[15,4096]{1,0:T(8,128)(2,1)S(1)}, u32[]{:S(2)}, u32[]{:S(2)}) collective-permute-start(bf16[15,4096]{1,0:T(8,128)(2,1)S(1)} %slice.340), channel_id=1, source_target_pairs={{0,1},{1,2},{2,3},{3,4},{4,5},{5,6},{6,7},{7,8},{8,9},{9,10},{10,1... | collective-permute-start | bytes 368648 | tf_op jit(solution)/shard_map/ppermute | solution.py:17
  160.9 8.0 %copy-start.5 = (bf16[384,1,1024]{2,0,1:T(8,128)(2,1)S(1)}, bf16[384,1,1024]{2,0,1:T(8,128)(2,1)}, u32[]{:S(2)}) copy-start(bf16[384,1,1024]{2,0,1:T(8,128)(2,1)} %fusion.56) | copy-start | bytes 2359300
  160.9 8.0 %copy-start.6 = (bf16[384,1,1024]{2,0,1:T(8,128)(2,1)S(1)}, bf16[384,1,1024]{2,0,1:T(8,128)(2,1)}, u32[]{:S(2)}) copy-start(bf16[384,1,1024]{2,0,1:T(8,128)(2,1)} %get-tuple-element.8) | copy-start | bytes 2359300
  160.9 8.0 %copy-start.7 = (bf16[384,1,1024]{2,0,1:T(8,128)(2,1)S(1)}, bf16[384,1,1024]{2,0,1:T(8,128)(2,1)}, u32[]{:S(2)}) copy-start(bf16[384,1,1024]{2,0,1:T(8,128)(2,1)} %get-tuple-element.9) | copy-start | bytes 2359300
  160.9 8.0 %copy-start.8 = (bf16[384,1,1024]{2,0,1:T(8,128)(2,1)S(1)}, bf16[384,1,1024]{2,0,1:T(8,128)(2,1)}, u32[]{:S(2)}) copy-start(bf16[384,1,1024]{2,0,1:T(8,128)(2,1)} %get-tuple-element.10) | copy-start | bytes 2359300
  177.1 2.6 %copy-start = (f32[4,48,8,1024]{3,2,0,1:T(8,128)}, f32[4,48,8,1024]{3,2,0,1:T(8,128)S(1)}, u32[]{:S(2)}) copy-start(f32[4,48,8,1024]{3,2,0,1:T(8,128)S(1)} %copy.14) | copy-start | bytes 18874372
  181.3 1.7 copy-start.3
  183.0 47.0 %collective-permute-start.1 = (bf16[15,4096]{1,0:T(8,128)(2,1)S(1)}, bf16[15,4096]{1,0:T(8,128)(2,1)S(1)}, u32[]{:S(2)}, u32[]{:S(2)}) collective-permute-start(bf16[15,4096]{1,0:T(8,128)(2,1)S(1)} %slice.371), channel_id=1, source_target_pairs={{0,1},{1,2},{2,3},{3,4},{4,5},{5,6},{6,7},{7,8},{8,9},{9,10},{10,1... | collective-permute-start | bytes 368648 | tf_op jit(solution)/shard_map/ppermute | solution.py:17
  222.0 7.9 %copy-start.4 = (bf16[384,4096]{1,0:T(8,128)(2,1)S(1)}, bf16[384,4096]{1,0:T(8,128)(2,1)}, u32[]{:S(2)}) copy-start(bf16[384,4096]{1,0:T(8,128)(2,1)} %copy-done.3) | copy-start | bytes 9437188
  230.9 5.4 %slice-start.2 = ((s8[8388608]{0:T(1024)(128)(4,1)}), s8[4194304]{0:T(1024)(128)(4,1)S(1)}, s32[]{:S(2)}) async-start(s8[8388608]{0:T(1024)(128)(4,1)} %bitcast.44), calls=%async_computation.6 | async-start | bytes 8388608
  233.7 2.6 %slice-start.3 = ((s8[8388608]{0:T(1024)(128)(4,1)}), s8[4194304]{0:T(1024)(128)(4,1)S(1)}, s32[]{:S(2)}) async-start(s8[8388608]{0:T(1024)(128)(4,1)} %bitcast.44), calls=%async_computation.7 | async-start | bytes 8388608
  236.3 7.0 %slice-start = ((s8[6291456]{0:T(1024)(128)(4,1)}), s8[4194304]{0:T(1024)(128)(4,1)S(1)}, s32[]{:S(2)}) async-start(s8[6291456]{0:T(1024)(128)(4,1)} %bitcast.38), calls=%async_computation.4 | async-start | bytes 8388608
  236.3 6.9 %slice-start.1 = ((s8[6291456]{0:T(1024)(128)(4,1)}), s8[2097152]{0:T(1024)(128)(4,1)S(1)}, s32[]{:S(2)}) async-start(s8[6291456]{0:T(1024)(128)(4,1)} %bitcast.38), calls=%async_computation.5 | async-start | bytes 4194304
Sparse Core Ops, SparseCore 0:
  8.9 44.9 all-gather.8
  55.5 44.4 all-gather.12
  101.6 59.2 all-gather.10
  162.3 59.6 all-gather.14
